TPU v7x, 512 devices: a whole 4x4x16 slice. The times are simulated.
512 devices in a mesh: ep: 128 (over z, x, core), tp: 4 (over y).
Axes of the slice: x: 4, y: 4, z: 16, core: 2. Of those that a mesh axis runs over, the one named last changes fastest.
Arguments:
- hidden_in: bfloat16 [2048, 1024], P('ep', 'tp'), may hold values from -40 to 40
- norm_gain_attn: float32 [1024], replicated, may hold values from 0.1 to 1.9
- query_weight: bfloat16 [1024, 512], P(None, 'tp'), may hold values from -0.1875 to 0.1875
- key_weight: bfloat16 [1024, 512], P(None, 'tp'), may hold values from -0.1875 to 0.1875
- value_weight: bfloat16 [1024, 512], P(None, 'tp'), may hold values from -0.1875 to 0.1875
- query_gain: float32 [128], replicated, may hold values from 1 to 1.6
- key_gain: float32 [128], replicated, may hold values from 1 to 1.6
- lambda_head: float32 [4], P('tp'), may hold values from 0.3 to 0.8
- sub_gain: float32 [128], replicated, may hold values from 0.1 to 1.9
- out_weight: bfloat16 [512, 1024], P('tp'), may hold values from -0.25 to 0.25
- cache_key: bfloat16 [2048, 256, 512], P('ep', None, 'tp'), may hold values from -8 to 8
- cache_value: bfloat16 [2048, 256, 512], P('ep', None, 'tp'), may hold values from -6 to 6
- lengths: int32 [2048], P('ep'), may hold values from 1 to 256
- norm_gain_mix: float32 [1024], P('tp'), may hold values from 0.1 to 1.9
- route_ids: int32 [2048, 6], P('ep'), may hold values from 0 to 127, all different within a row; in each aligned block of 16 rows (0 to 15, 16 to 31, ...) at most 2 rows name the same one
- route_logits: float32 [2048, 6], P('ep'), may hold values from -4 to 4
- expert_gate: bfloat16 [128, 1024, 1024], P('ep', None, 'tp'), may hold values from -0.5 to 0.5
- expert_up: bfloat16 [128, 1024, 1024], P('ep', None, 'tp'), may hold values from -0.5 to 0.5
- expert_down: bfloat16 [128, 1024, 1024], P('ep', 'tp'), may hold values from -0.046875 to 0.046875
- dense_gate: bfloat16 [1024, 2048], P('tp', 'ep'), may hold values from -0.1875 to 0.1875
- dense_up: bfloat16 [1024, 2048], P('tp', 'ep'), may hold values from -0.1875 to 0.1875
- dense_down: bfloat16 [2048, 1024], P('ep', 'tp'), may hold values from -0.125 to 0.125
- branch_gate: float32 [1024], P('tp'), may hold values from -0.1875 to 0.1875
Outputs:
- layer_out: bfloat16 [2048, 1024], P('ep', 'tp')
- key_rows: bfloat16 [2048, 512], P('ep', 'tp')
- value_rows: bfloat16 [2048, 512], P('ep', 'tp')
Inputs may be any that keep to these rules, and one draw needn't show every extreme that they name: `route_ids`: each row names 6 different experts. Among the rows of one index of ep (aligned blocks of 16 rows) no expert is named by more than 2 rows, and in some blocks one expert is named by exactly 2.
All inputs are finite; a program needn't handle non-finite values.
Results may differ from a plain program's by a relative error of at most 0.0075.
Values may be sent and summed in bfloat16 or wider, within the bound.
No kernel may reach another device: no remote copies, remote signals or barrier semaphores. Data moves between devices by JAX's collectives and lax.ppermute only.
A program may use at most 64 MiB of HBM per device.

v0:
```python
import math
import jax
import jax.numpy as jnp
from jax import lax
from jax.sharding import Mesh
from jax.sharding import PartitionSpec as P

EP = ("ep_0", "ep_1", "ep_2")
EPSILON = 1e-06
CLAMP_LIMIT = 7.0
SWISH_ALPHA = 1.702
OUT_SCALE = 0.2 + 0.6 * math.exp(-0.6)


def laid_out(blocks, dim):
    blocks = jnp.moveaxis(blocks, 0, dim)
    dims = blocks.shape
    return blocks.reshape(*dims[:dim], dims[dim] * dims[dim + 1], *dims[dim + 2 :])


def from_everyone(x, axis):
    copies = jnp.broadcast_to(x, (lax.axis_size(axis), *x.shape))
    return lax.all_to_all(copies, axis, split_axis=0, concat_axis=0, tiled=True)


def collect(x, axis, dim):
    return laid_out(from_everyone(x, axis), dim)


def cut_along(x, dim, length):
    dims = x.shape
    blocks = x.reshape(*dims[:dim], length, dims[dim] // length, *dims[dim + 1 :])
    return jnp.moveaxis(blocks, dim, 0)


def summed_on_arrival(x, axis, dim):
    length = lax.axis_size(axis)
    blocks = lax.all_to_all(cut_along(x, dim, length), axis, 0, 0, tiled=True)
    return jnp.sum(blocks, axis=0)


def taken_together(x, axis):
    return from_everyone(x, axis).sum(axis=0)


def together(arrays, axis):
    ends = [0]
    for a in arrays:
        ends.append(ends[-1] + a.size)
    subtotal = taken_together(jnp.concatenate([a.ravel() for a in arrays]), axis)
    return tuple((subtotal[b:e].reshape(a.shape) for a, b, e in zip(arrays, ends, ends[1:])))


def gather_turned(arrays, axis, dims):
    turned = [jnp.moveaxis(a, dim, 0) for a, dim in zip(arrays, dims)]
    both = jnp.concatenate([t.reshape(len(t), -1) for t in turned], axis=1)
    whole, at, done = (lax.all_gather(both, axis, axis=0, tiled=True), 0, [])
    for t, dim in zip(turned, dims):
        section = whole[:, at : at + t[0].size].reshape(-1, *t.shape[1:])
        done.append(jnp.moveaxis(section, 0, dim))
        at += t[0].size
    return tuple(done)


def stacked_from(x, axes, sequence):
    blocks = x[None]
    for k in sequence:
        blocks = lax.all_gather(blocks, axes[k], axis=0, tiled=True)
    block = [lax.axis_size(axes[k]) for k in reversed(sequence)]
    blocks = blocks.reshape(*block, *x.shape)
    turned = sorted(range(len(sequence)), key=lambda place: sequence[len(sequence) - 1 - place])
    return blocks.transpose(*turned, *range(len(sequence), blocks.ndim)).reshape(-1, *x.shape)


def whole_of(x, axes, sequence, dim):
    return laid_out(stacked_from(x, axes, sequence), dim)


def rms_scale(values, scale_gain):
    mean_square = jnp.mean(values * values, axis=-1, keepdims=True)
    return values * lax.rsqrt(mean_square + EPSILON) * scale_gain


def clamped_unit(gate_pre, up_pre):
    gate_cut = jnp.minimum(gate_pre, CLAMP_LIMIT)
    up_cut = jnp.clip(up_pre, -CLAMP_LIMIT, CLAMP_LIMIT)
    return (up_cut + 1.0) * gate_cut * jax.nn.sigmoid(SWISH_ALPHA * gate_cut)


def attend(
    normed,
    query_weight,
    key_weight,
    value_weight,
    query_gain,
    key_gain,
    lambda_head,
    sub_gain,
    cache_key,
    cache_value,
    lengths,
):
    seq_count = normed.shape[0]
    head_count = lambda_head.shape[0]
    qk_size = query_gain.shape[0] // 2
    val_size = value_weight.shape[1] // head_count
    cache_len = cache_key.shape[1]
    scale_factor = qk_size ** (-0.5)
    query_pre = jnp.dot(normed, query_weight, preferred_element_type=jnp.float32)
    query_rows = rms_scale(
        query_pre.reshape(seq_count, head_count, 2, qk_size), query_gain.reshape(2, qk_size)
    ).astype(jnp.bfloat16)
    key_pre = jnp.dot(normed, key_weight, preferred_element_type=jnp.float32)
    key_rows = rms_scale(
        key_pre.reshape(seq_count, head_count, 2, qk_size), key_gain.reshape(2, qk_size)
    ).astype(jnp.bfloat16)
    value_rows = jnp.dot(normed, value_weight, preferred_element_type=jnp.float32).astype(
        jnp.bfloat16
    )
    key_past = cache_key.reshape(seq_count, cache_len, head_count, 2, qk_size)
    past_score = (
        jnp.einsum("shmd,sjhmd->shmj", query_rows, key_past, preferred_element_type=jnp.float32)
        * scale_factor
    )
    own_score = (
        jnp.einsum("shmd,shmd->shm", query_rows, key_rows, preferred_element_type=jnp.float32)
        * scale_factor
    )
    valid_mask = lax.iota(jnp.int32, cache_len)[None, :] < lengths[:, None]
    past_exp = jnp.where(valid_mask[:, None, None, :], jnp.exp(past_score), 0.0)
    own_exp = jnp.exp(own_score)
    denominator = jnp.sum(past_exp, axis=-1) + own_exp
    past_prob = past_exp / denominator[..., None]
    own_prob = own_exp / denominator
    weight_past = (past_prob[:, :, 0] - lambda_head[None, :, None] * past_prob[:, :, 1]).astype(
        jnp.bfloat16
    )
    weight_own = (own_prob[:, :, 0] - lambda_head[None, :] * own_prob[:, :, 1]).astype(jnp.bfloat16)
    value_past = cache_value.reshape(seq_count, cache_len, head_count, val_size)
    head_mix = jnp.einsum(
        "shj,sjhe->she", weight_past, value_past, preferred_element_type=jnp.float32
    )
    own_value = value_rows.reshape(seq_count, head_count, val_size).astype(jnp.float32)
    head_mix = head_mix + weight_own.astype(jnp.float32)[..., None] * own_value
    head_out = (rms_scale(head_mix, sub_gain) * OUT_SCALE).astype(jnp.bfloat16)
    return (
        head_out.reshape(seq_count, head_count * val_size),
        key_rows.reshape(seq_count, -1),
        value_rows,
    )


def body(
    hidden_in,
    norm_gain_attn,
    query_weight,
    key_weight,
    value_weight,
    query_gain,
    key_gain,
    lambda_head,
    sub_gain,
    out_weight,
    cache_key,
    cache_value,
    lengths,
    norm_gain_mix,
    route_ids,
    route_logits,
    expert_gate,
    expert_up,
    expert_down,
    dense_gate,
    dense_up,
    dense_down,
    branch_gate,
):
    seq_count, top_count = route_ids.shape
    full_rows = collect(hidden_in, "tp", 1)
    width_total = full_rows.shape[1]
    normed = rms_scale(full_rows.astype(jnp.float32), norm_gain_attn).astype(jnp.bfloat16)
    head_out, key_rows, value_rows = attend(
        normed,
        query_weight,
        key_weight,
        value_weight,
        query_gain,
        key_gain,
        lambda_head,
        sub_gain,
        cache_key,
        cache_value,
        lengths,
    )
    head_terms = jnp.dot(head_out, out_weight, preferred_element_type=jnp.float32)
    attn_part = summed_on_arrival(head_terms, "tp", 1)
    residual = hidden_in.astype(jnp.float32) + attn_part
    square_sum, gate_raw = together(
        (
            jnp.sum(residual * residual, axis=1),
            jnp.sum(residual * (norm_gain_mix * branch_gate)[None, :], axis=1),
        ),
        "tp",
    )
    inverse = lax.rsqrt(square_sum / width_total + EPSILON)
    mix_float = residual * inverse[:, None] * norm_gain_mix[None, :]
    gate_logit = gate_raw * inverse
    branch_weight = jax.nn.sigmoid(gate_logit)[:, None]
    mix_rows = mix_float.astype(jnp.bfloat16)
    route_weight = jax.nn.softmax(route_logits, axis=1)
    experts = lax.axis_size(EP) * expert_gate.shape[0]
    capacity = min(seq_count, 2 * ((seq_count * top_count + experts - 1) // experts))
    flat_ids = route_ids.reshape(-1)
    one_hot = (flat_ids[:, None] == lax.iota(jnp.int32, experts)[None, :]).astype(jnp.int32)
    route_rank = jnp.sum((jnp.cumsum(one_hot, axis=0) - one_hot) * one_hot, axis=1)
    slot_index = flat_ids * capacity + route_rank
    select_matrix = (
        lax.iota(jnp.int32, experts * capacity)[:, None] == slot_index[None, :]
    ).astype(jnp.bfloat16)
    route_rows = jnp.repeat(mix_rows, top_count, axis=0)
    placed = jnp.dot(select_matrix, route_rows, preferred_element_type=jnp.float32)
    arrived = collect(
        lax.all_to_all(
            placed.astype(jnp.bfloat16).reshape(experts, capacity, mix_rows.shape[1]),
            EP,
            split_axis=0,
            concat_axis=0,
            tiled=True,
        ),
        "tp",
        2,
    )
    source_count, item_count, width_now = arrived.shape
    flat_rows = arrived.reshape(source_count * item_count, width_now)
    gate_pre = jnp.dot(flat_rows, expert_gate[0], preferred_element_type=jnp.float32)
    up_pre = jnp.dot(flat_rows, expert_up[0], preferred_element_type=jnp.float32)
    activation = clamped_unit(gate_pre, up_pre).astype(jnp.bfloat16)
    partial_out = jnp.dot(activation, expert_down[0], preferred_element_type=jnp.float32)
    partial_out = partial_out.reshape(source_count, item_count, width_now)
    summed = summed_on_arrival(partial_out, "tp", 2).astype(jnp.bfloat16)
    returned = lax.all_to_all(summed, EP, split_axis=0, concat_axis=0, tiled=True)
    local_width = returned.shape[2]
    route_out = jnp.dot(
        select_matrix.T,
        returned.reshape(experts * capacity, local_width),
        preferred_element_type=jnp.float32,
    )
    routed = jnp.sum(
        route_out.reshape(seq_count, top_count, local_width) * route_weight[:, :, None], axis=1
    )
    pieces = gather_turned((dense_gate, dense_up), EP, (1, 1))
    gate_block = jnp.dot(mix_rows, pieces[0], preferred_element_type=jnp.float32)
    up_block = jnp.dot(mix_rows, pieces[1], preferred_element_type=jnp.float32)
    gate_full, up_full = together((gate_block, up_block), "tp")
    own_act = (jax.nn.silu(gate_full) * up_full).astype(jnp.bfloat16)
    dense_result = jnp.dot(
        own_act, whole_of(dense_down, EP, (1, 0, 2), 0), preferred_element_type=jnp.float32
    )
    layer_out = (residual + routed + branch_weight * dense_result).astype(jnp.bfloat16)
    return (layer_out, key_rows, value_rows)


def solution(mesh):
    split = Mesh(mesh.devices.reshape(16, 4, 2, mesh.shape["tp"]), ("ep_0", "ep_1", "ep_2", "tp"))
    in_specs = (
        P(EP, "tp"),
        P(),
        P(None, "tp"),
        P(None, "tp"),
        P(None, "tp"),
        P(),
        P(),
        P("tp"),
        P(),
        P("tp", None),
        P(EP, None, "tp"),
        P(EP, None, "tp"),
        P(EP),
        P("tp"),
        P(EP, None),
        P(EP, None),
        P(EP, None, "tp"),
        P(EP, None, "tp"),
        P(EP, "tp", None),
        P("tp", EP),
        P("tp", EP),
        P(EP, "tp"),
        P("tp"),
    )
    out_specs = (P(EP, "tp"), P(EP, "tp"), P(EP, "tp"))
    return jax.shard_map(body, mesh=split, in_specs=in_specs, out_specs=out_specs, check_vma=False)
```

profile of v0, /device:TPU:32, one launch (start us, length us, event | category | flops | bytes accessed | tf_op | source)
XLA Modules:
  0.0 202.3 jit_solution(13070366693453311810)
XLA Ops:
  7.2 1.4 broadcast_in_dim.25
  8.6 4.5 %all-to-all-start = ((bf16[4,16,256]{2,1,0:T(8,128)(2,1)}), bf16[4,16,256]{2,1,0:T(8,128)(2,1)S(1)}, u32[]{:S(2)}, u32[]{:S(2)}) async-start(bf16[4,16,256]{2,1,0:T(8,128)(2,1)} %broadcast_in_dim.25), calls=%async_computation | async-start | bytes 65536 | tf_op jit(solution)/shard_map/all_to_all | solution.py:23
  13.1 1.3 pad_maximum_fusion.1
  14.5 0.8 copy.83
  15.4 0.7 iota_compare_fusion.4
  16.1 0.7 mul.280
  16.9 0.7 mul.289
  17.6 1.5 copy.81
  19.7 0.2 copy.104
  21.2 0.2 fusion.22
  21.5 0.2 fusion.25
  22.0 0.2 fusion.23
  22.2 1.2 multiply_reduce_fusion.2
  23.5 0.8 convolution_bitcast_fusion.3
  24.3 4.8 %all-to-all-start.1 = ((f32[4,16,256]{2,1,0:T(8,128)}), f32[4,16,256]{2,1,0:T(8,128)S(1)}, u32[]{:S(2)}, u32[]{:S(2)}) async-start(f32[4,16,256]{2,1,0:T(8,128)} %convolution_bitcast_fusion.3), calls=%async_computation.1 | async-start | bytes 131072 | tf_op jit(solution)/shard_map/all_to_all | solution.py:38
  29.1 0.2 select_reduce_fusion
  29.3 5.4 %all-to-all-done.1 = f32[4,16,256]{2,1,0:T(8,128)S(1)} async-done(((f32[4,16,256]{2,1,0:T(8,128)}), f32[4,16,256]{2,1,0:T(8,128)S(1)}, u32[]{:S(2)}, u32[]{:S(2)}) %all-to-all-start.1) | async-done | bytes 65568 | tf_op jit(solution)/shard_map/all_to_all | solution.py:38
  34.9 0.6 broadcast_in_dim.27
  35.5 3.2 %all-to-all-start.2 = ((f32[4,1,32]{2,1,0:T(1,128)}), f32[4,1,32]{2,1,0:T(1,128)S(1)}, u32[]{:S(2)}, u32[]{:S(2)}) async-start(f32[4,1,32]{2,1,0:T(1,128)} %broadcast_in_dim.27), calls=%async_computation.2 | async-start | bytes 4096 | tf_op jit(solution)/shard_map/all_to_all | solution.py:23
  38.8 5.2 %all-to-all-done.2 = f32[4,1,32]{2,1,0:T(1,128)S(1)} async-done(((f32[4,1,32]{2,1,0:T(1,128)}), f32[4,1,32]{2,1,0:T(1,128)S(1)}, u32[]{:S(2)}, u32[]{:S(2)}) %all-to-all-start.2) | async-done | bytes 544 | tf_op jit(solution)/shard_map/all_to_all | solution.py:23
  44.2 0.2 convolution_convert_fusion
  44.4 36.1 %all_to_all.42 = bf16[128,2,256]{2,1,0:T(2,128)(2,1)S(1)} all-to-all(bf16[128,2,256]{2,1,0:T(2,128)(2,1)S(1)} %reshape.305), channel_id=1, replica_groups=mesh['ep_0'=16,'ep_1'=4,'ep_2'=2,'tp'=4] {'ep_0','ep_1','ep_2'}, dimensions={0} | all-to-all | bytes 262144 | tf_op jit(solution)/shard_map/all_to_all | solution.py:223
  80.5 1.1 broadcast_in_dim.29
  81.6 3.6 %all-to-all-start.4 = ((bf16[4,128,2,256]{3,2,1,0:T(2,128)(2,1)}), bf16[4,128,2,256]{3,2,1,0:T(2,128)(2,1)S(1)}, u32[]{:S(2)}, u32[]{:S(2)}) async-start(bf16[4,128,2,256]{3,2,1,0:T(2,128)(2,1)} %broadcast_in_dim.29), calls=%async_computation.4 | async-start | bytes 1048576 | tf_op jit(solution)/shard_map/all_to_all | solution.py:23
  85.2 0.2 copy.107
  85.4 9.8 %all-to-all-done.4 = bf16[4,128,2,256]{3,2,1,0:T(2,128)(2,1)S(1)} async-done(((bf16[4,128,2,256]{3,2,1,0:T(2,128)(2,1)}), bf16[4,128,2,256]{3,2,1,0:T(2,128)(2,1)S(1)}, u32[]{:S(2)}, u32[]{:S(2)}) %all-to-all-start.4) | async-done | bytes 524320 | tf_op jit(solution)/shard_map/all_to_all | solution.py:23
  95.2 0.7 copy.85
  96.0 0.3 convolution_minimum_fusion
  96.3 0.3 fusion.3
  96.7 0.3 convolution_bitcast_fusion
  97.1 1.1 copy.88
  98.1 3.5 %all-to-all-start.5 = ((f32[4,128,2,256]{3,1,2,0:T(8,128)}), f32[4,128,2,256]{3,1,2,0:T(8,128)S(1)}, u32[]{:S(2)}, u32[]{:S(2)}) async-start(f32[4,128,2,256]{3,1,2,0:T(8,128)} %copy.88), calls=%async_computation.5 | async-start | bytes 2097152 | tf_op jit(solution)/shard_map/all_to_all | solution.py:38
  101.7 11.9 %all-gather = bf16[64,256]{1,0:T(8,128)(2,1)S(1)} all-gather(bf16[16,256]{1,0:T(8,128)(2,1)S(1)} %copy-done.8), channel_id=2, replica_groups=mesh['ep_0'=16,'ep_1'=4,'ep_2'=2,'tp'=4] {'ep_1'}, dimensions={0}, use_global_device_ids=true | all-gather | bytes 40960 | tf_op jit(solution)/shard_map/all_gather | solution.py:68
  113.6 31.7 %all_gather.14 = bf16[64,16,256]{2,1,0:T(8,128)(2,1)} all-gather(bf16[4,16,256]{2,1,0:T(8,128)(2,1)S(1)} %bitcast.104), channel_id=1, replica_groups=mesh['ep_0'=16,'ep_1'=4,'ep_2'=2,'tp'=4] {'ep_0'}, dimensions={0}, use_global_device_ids=true | all-gather | bytes 557056 | tf_op jit(solution)/shard_map/all_gather | solution.py:68
  145.4 0.8 copy.90
  146.2 8.6 %all-to-all-start.6 = ((bf16[128,2,256]{2,1,0:T(2,128)(2,1)}), bf16[128,2,256]{2,1,0:T(2,128)(2,1)S(1)}, u32[]{:S(2)}, u32[]{:S(2)}) async-start(bf16[128,2,256]{2,1,0:T(2,128)(2,1)} %copy.90), calls=%async_computation.6 | async-start | bytes 262144 | tf_op jit(solution)/shard_map/all_to_all | solution.py:241
  154.9 6.9 %all-gather.4.cloned.1.call-done = bf16[2048,512]{1,0:T(8,128)(2,1)} async-done(((bf16[16,512]{1,0:T(8,128)(2,1)}), bf16[2048,512]{1,0:T(8,128)(2,1)}) %all-gather.4.cloned.1.call-update) | async-done | bytes 2097168 | tf_op jit(solution)/shard_map/all_gather | solution.py:57
  161.8 1.6 convolution_bitcast_fusion.2
  163.4 1.6 convolution_bitcast_fusion.1
  165.1 6.8 %all-to-all-done.6 = bf16[128,2,256]{2,1,0:T(2,128)(2,1)S(1)} async-done(((bf16[128,2,256]{2,1,0:T(2,128)(2,1)}), bf16[128,2,256]{2,1,0:T(2,128)(2,1)S(1)}, u32[]{:S(2)}, u32[]{:S(2)}) %all-to-all-start.6) | async-done | bytes 131104 | tf_op jit(solution)/shard_map/all_to_all | solution.py:241
  171.9 1.5 broadcast_in_dim.30
  173.5 4.7 %all-to-all-start.7 = ((f32[4,1,65536]{2,1,0:T(1,128)}), f32[4,1,65536]{2,1,0:T(1,128)S(1)}, u32[]{:S(2)}, u32[]{:S(2)}) async-start(f32[4,1,65536]{2,1,0:T(1,128)} %broadcast_in_dim.30), calls=%async_computation.7 | async-start | bytes 2097152 | tf_op jit(solution)/shard_map/all_to_all | solution.py:23
  178.5 0.6 multiply_convert_fusion.6
  179.1 1.2 all-gather.6.cloned.1.call-done
  180.4 1.3 copy.93
  181.9 11.6 %all-to-all-done.7 = f32[4,1,65536]{2,1,0:T(1,128)S(1)} async-done(((f32[4,1,65536]{2,1,0:T(1,128)}), f32[4,1,65536]{2,1,0:T(1,128)S(1)}, u32[]{:S(2)}, u32[]{:S(2)}) %all-to-all-start.7) | async-done | bytes 1048608 | tf_op jit(solution)/shard_map/all_to_all | solution.py:23
  193.5 1.0 reduce_sum.139
  194.6 0.9 fusion.6
  (91 shorter events, 3.2 us)
Async XLA Ops:
  7.2 14.8 %copy-start = (bf16[16,256,128]{2,1,0:T(8,128)(2,1)S(1)}, bf16[16,256,128]{2,1,0:T(8,128)(2,1)}, u32[]{:S(2)}) copy-start(bf16[16,256,128]{2,1,0:T(8,128)(2,1)} %param.34) | copy-start | bytes 3145732
  7.2 12.6 %copy-start.5 = (bf16[128,1024]{1,0:T(8,128)(2,1)S(1)}, bf16[128,1024]{1,0:T(8,128)(2,1)}, u32[]{:S(2)}) copy-start(bf16[128,1024]{1,0:T(8,128)(2,1)} %param.32) | copy-start | bytes 786436
  7.2 13.1 %copy-start.10 = (f32[1024]{0:T(1024)S(1)}, f32[1024]{0:T(1024)}, u32[]{:S(2)}) copy-start(f32[1024]{0:T(1024)} %param.24) | copy-start | bytes 12292
  7.2 13.1 %copy-start.3 = (bf16[1024,128]{1,0:T(8,128)(2,1)S(1)}, bf16[1024,128]{1,0:T(8,128)(2,1)}, u32[]{:S(2)}) copy-start(bf16[1024,128]{1,0:T(8,128)(2,1)} %param.25) | copy-start | bytes 786436
  7.2 13.4 %copy-start.4 = (bf16[1024,128]{1,0:T(8,128)(2,1)S(1)}, bf16[1024,128]{1,0:T(8,128)(2,1)}, u32[]{:S(2)}) copy-start(bf16[1024,128]{1,0:T(8,128)(2,1)} %param.26) | copy-start | bytes 786436
  8.6 11.4 %all-to-all-start = ((bf16[4,16,256]{2,1,0:T(8,128)(2,1)}), bf16[4,16,256]{2,1,0:T(8,128)(2,1)S(1)}, u32[]{:S(2)}, u32[]{:S(2)}) async-start(bf16[4,16,256]{2,1,0:T(8,128)(2,1)} %broadcast_in_dim.25), calls=%async_computation | async-start | bytes 65536 | tf_op jit(solution)/shard_map/all_to_all | solution.py:23
  13.1 148.7 %all-gather.4.cloned.1.call-start = ((), (), s32[]{:S(2)}) async-start(), calls=%async_computation.8 | async-start | bytes 2113536 | tf_op jit(solution)/shard_map/all_gather | solution.py:57
  19.9 3.5 %copy-start.13 = (f32[128]{0:T(128)S(1)}, f32[128]{0:T(128)}, u32[]{:S(2)}) copy-start(f32[128]{0:T(128)} %param.31) | copy-start | bytes 1540
  20.2 9.1 %copy-start.11 = (f32[256]{0:T(256)S(1)}, f32[256]{0:T(256)}, u32[]{:S(2)}) copy-start(f32[256]{0:T(256)} %param.36) | copy-start | bytes 3076
  20.2 9.1 %copy-start.12 = (f32[256]{0:T(256)S(1)}, f32[256]{0:T(256)}, u32[]{:S(2)}) copy-start(f32[256]{0:T(256)} %param.45) | copy-start | bytes 3076
  20.3 14.4 %copy-start.6 = (bf16[16,256]{1,0:T(8,128)(2,1)S(1)}, bf16[16,256]{1,0:T(8,128)(2,1)}, u32[]{:S(2)}) copy-start(bf16[16,256]{1,0:T(8,128)(2,1)} %param.23) | copy-start | bytes 24580
  21.9 63.3 %copy-start.1 = (bf16[1,256,1024]{2,1,0:T(8,128)(2,1)S(1)}, bf16[1,256,1024]{2,1,0:T(8,128)(2,1)}, u32[]{:S(2)}) copy-start(bf16[1,256,1024]{2,1,0:T(8,128)(2,1)} %param.41) | copy-start | bytes 1572868
  23.4 62.0 %copy-start.9 = (bf16[16,128]{1,0:T(8,128)(2,1)}, bf16[16,128]{1,0:T(8,128)(2,1)S(1)}, u32[]{:S(2)}) copy-start(bf16[16,128]{1,0:T(8,128)(2,1)S(1)} %get-tuple-element.18) | copy-start | bytes 12292
  24.3 10.4 %all-to-all-start.1 = ((f32[4,16,256]{2,1,0:T(8,128)}), f32[4,16,256]{2,1,0:T(8,128)S(1)}, u32[]{:S(2)}, u32[]{:S(2)}) async-start(f32[4,16,256]{2,1,0:T(8,128)} %convolution_bitcast_fusion.3), calls=%async_computation.1 | async-start | bytes 131072 | tf_op jit(solution)/shard_map/all_to_all | solution.py:38
  35.5 8.4 %all-to-all-start.2 = ((f32[4,1,32]{2,1,0:T(1,128)}), f32[4,1,32]{2,1,0:T(1,128)S(1)}, u32[]{:S(2)}, u32[]{:S(2)}) async-start(f32[4,1,32]{2,1,0:T(1,128)} %broadcast_in_dim.27), calls=%async_computation.2 | async-start | bytes 4096 | tf_op jit(solution)/shard_map/all_to_all | solution.py:23
  81.6 14.4 %copy-start.2 = (bf16[1,1024,256]{2,1,0:T(8,128)(2,1)S(1)}, bf16[1,1024,256]{2,1,0:T(8,128)(2,1)}, u32[]{:S(2)}) copy-start(bf16[1,1024,256]{2,1,0:T(8,128)(2,1)} %param.39) | copy-start | bytes 1572868
  81.6 13.6 %all-to-all-start.4 = ((bf16[4,128,2,256]{3,2,1,0:T(2,128)(2,1)}), bf16[4,128,2,256]{3,2,1,0:T(2,128)(2,1)S(1)}, u32[]{:S(2)}, u32[]{:S(2)}) async-start(bf16[4,128,2,256]{3,2,1,0:T(2,128)(2,1)} %broadcast_in_dim.29), calls=%async_computation.4 | async-start | bytes 1048576 | tf_op jit(solution)/shard_map/all_to_all | solution.py:23
  85.4 10.9 %copy-start.15 = (bf16[1,1024,256]{2,1,0:T(8,128)(2,1)S(1)}, bf16[1,1024,256]{2,1,0:T(8,128)(2,1)}, u32[]{:S(2)}) copy-start(bf16[1,1024,256]{2,1,0:T(8,128)(2,1)} %param.40) | copy-start | bytes 1572868
  97.0 4.6 %copy-start.8 = (bf16[16,256]{1,0:T(8,128)(2,1)S(1)}, bf16[16,256]{1,0:T(8,128)(2,1)}, u32[]{:S(2)}) copy-start(bf16[16,256]{1,0:T(8,128)(2,1)} %param.44) | copy-start | bytes 24580
  98.1 47.2 %all-to-all-start.5 = ((f32[4,128,2,256]{3,1,2,0:T(8,128)}), f32[4,128,2,256]{3,1,2,0:T(8,128)S(1)}, u32[]{:S(2)}, u32[]{:S(2)}) async-start(f32[4,128,2,256]{3,1,2,0:T(8,128)} %copy.88), calls=%async_computation.5 | async-start | bytes 2097152 | tf_op jit(solution)/shard_map/all_to_all | solution.py:38
  101.6 78.7 %all-gather.6.cloned.1.call-start = ((), (), s32[]{:S(2)}) async-start(), calls=%async_computation.9 | async-start | bytes 1572864 | tf_op jit(solution)/shard_map/all_gather | solution.py:68
  146.2 25.7 %all-to-all-start.6 = ((bf16[128,2,256]{2,1,0:T(2,128)(2,1)}), bf16[128,2,256]{2,1,0:T(2,128)(2,1)S(1)}, u32[]{:S(2)}, u32[]{:S(2)}) async-start(bf16[128,2,256]{2,1,0:T(2,128)(2,1)} %copy.90), calls=%async_computation.6 | async-start | bytes 262144 | tf_op jit(solution)/shard_map/all_to_all | solution.py:241
  165.0 13.2 %copy-start.7 = (f32[16,6]{0,1:T(8,128)S(1)}, f32[16,6]{0,1:T(8,128)}, u32[]{:S(2)}) copy-start(f32[16,6]{0,1:T(8,128)} %param.38) | copy-start | bytes 1156
  165.1 13.4 %copy-start.14 = (f32[128]{0:T(128)S(1)}, f32[128]{0:T(128)}, u32[]{:S(2)}) copy-start(f32[128]{0:T(128)} %param.29) | copy-start | bytes 1540
  173.5 20.0 %all-to-all-start.7 = ((f32[4,1,65536]{2,1,0:T(1,128)}), f32[4,1,65536]{2,1,0:T(1,128)S(1)}, u32[]{:S(2)}, u32[]{:S(2)}) async-start(f32[4,1,65536]{2,1,0:T(1,128)} %broadcast_in_dim.30), calls=%async_computation.7 | async-start | bytes 2097152 | tf_op jit(solution)/shard_map/all_to_all | solution.py:23
Sparse Core Ops, SparseCore 0:
  17.0 144.7 all-gather.3
  163.9 16.4 all-gather.5
where the time goes:
time: 203 us; the launch traced here: 202 us
  blocking collectives  79.8 us (39%)
  waiting for transfers between devices  47 us (23%)
  starting transfers between devices  32.9 us (16%)
  between operations  15.2 us (7%)
  local copies, waits for them, and re-layouts  13.8 us (7%)
  matrix products  8.19 us (4%)
  other arithmetic  5.41 us (3%)
    all_gather x2, blocking collectives, stacked_from(): blocks = lax.all_gather(blocks, axes[k], axis=0, tiled=True)  43.6 us
    all_to_all x1, blocking collectives, body(): lax.all_to_all(placed.astype(jnp.bfloat16).reshape(experts, capacity, mix...  36.1 us
    all_to_all x4, waiting for transfers between devices, from_everyone(): return lax.all_to_all(copies, axis, split_axis=0, concat_axis=0, tiled=True)  26.5 us
    all_to_all x4, starting transfers between devices, from_everyone(): return lax.all_to_all(copies, axis, split_axis=0, concat_axis=0, tiled=True)  16 us
    all_to_all x1, starting transfers between devices, body(): lax.all_to_all(summed, EP, split_axis=0, concat_axis=0, tiled=True)  8.63 us
    all_to_all x2, starting transfers between devices, summed_on_arrival(): blocks = lax.all_to_all(cut_along(x, dim, length), axis, 0, 0, tiled=True)  8.31 us
    all_gather x1, waiting for transfers between devices, gather_turned(): whole, at, done = (lax.all_gather(both, axis, axis=0, tiled=True), 0, [])  6.94 us
    all_to_all x1, waiting for transfers between devices, body(): lax.all_to_all(summed, EP, split_axis=0, concat_axis=0, tiled=True)  6.83 us
  transfers between devices with their start and end apart: 9, of which 7 were waited for; matrix products, arithmetic and copies ran while one was open for 12% of the time, Pallas kernels for 0%

commit v1 on v0

--- a/solution.py
+++ b/solution.py
@@ -65,7 +65,8 @@
 def stacked_from(x, axes, sequence):
     blocks = x[None]
     for k in sequence:
-        blocks = lax.all_gather(blocks, axes[k], axis=0, tiled=True)
+        repeated = jnp.stack([blocks] * lax.axis_size(axes[k]))
+        blocks = jnp.concatenate(lax.all_to_all(repeated, axes[k], 0, 0), axis=0)
     block = [lax.axis_size(axes[k]) for k in reversed(sequence)]
     blocks = blocks.reshape(*block, *x.shape)
     turned = sorted(range(len(sequence)), key=lambda place: sequence[len(sequence) - 1 - place])

time: 203 us -> 273 us (1.34)
  waiting for transfers between devices: 47 us -> 149 us
  blocking collectives: 79.8 us -> 16.1 us
  starting transfers between devices: 32.9 us -> 62.5 us
    all_gather x1, waiting for transfers between devices: 6.94 us -> 54.1 us  [gather_turned(): whole, at, done = (lax.all_gather(both, axis, axis=0, tiled=True), 0, [])]
    all_to_all x0 -> x4, waiting for transfers between devices: none -> 44.4 us  [the longest x3 28 us: stacked_from(): blocks = jnp.concatenate(lax.all_to_all(repeated, axes[k], 0, 0), axis=0)]
    all_gather x2 -> x0, blocking collectives: 43.6 us -> none  [stacked_from(): blocks = lax.all_gather(blocks, axes[k], axis=0, tiled=True)]
    all_to_all x0 -> x4, starting transfers between devices: none -> 29.7 us  [the longest x1 19 us: body(): lax.all_to_all(placed.astype(jnp.bfloat16).reshape(experts, capacity, mix...]
    all_to_all x1, blocking collectives: 36.1 us -> 16.1 us  [summed_on_arrival(): blocks = lax.all_to_all(cut_along(x, dim, length), axis, 0, 0, tiled=True)]
    all_to_all x1, waiting for transfers between devices: 6.83 us -> 17 us  [body(): lax.all_to_all(summed, EP, split_axis=0, concat_axis=0, tiled=True)]
    all_to_all x1, starting transfers between devices: 8.63 us -> 12.2 us  [body(): lax.all_to_all(summed, EP, split_axis=0, concat_axis=0, tiled=True)]
    all_to_all x2 -> x1, starting transfers between devices: 8.31 us -> 4.93 us  [summed_on_arrival(): blocks = lax.all_to_all(cut_along(x, dim, length), axis, 0, 0, tiled=True)]
  transfers between devices with their start and end apart: 9 -> 11, of which waited for: 7 -> 9; matrix products, arithmetic and copies ran while one was open for 12% -> 7% of each run, Pallas kernels for 0% -> 0%
where the time goes in v1:
time: 273 us; the launch traced here: 272 us
  waiting for transfers between devices  149 us (55%)
  starting transfers between devices  62.5 us (23%)
  blocking collectives  16.1 us (6%)
  between operations  15.3 us (6%)
  local copies, waits for them, and re-layouts  14.8 us (5%)
  matrix products  8.22 us (3%)
  other arithmetic  5.79 us (2%)
    all_gather x1, waiting for transfers between devices, gather_turned(): whole, at, done = (lax.all_gather(both, axis, axis=0, tiled=True), 0, [])  54.1 us
    all_to_all x3, waiting for transfers between devices, stacked_from(): blocks = jnp.concatenate(lax.all_to_all(repeated, axes[k], 0, 0), axis=0)  28 us
    all_to_all x4, waiting for transfers between devices, from_everyone(): return lax.all_to_all(copies, axis, split_axis=0, concat_axis=0, tiled=True)  28 us
    all_to_all x1, starting transfers between devices, body(): lax.all_to_all(placed.astype(jnp.bfloat16).reshape(experts, capacity, mix...  19 us
    all_to_all x1, waiting for transfers between devices, body(): lax.all_to_all(summed, EP, split_axis=0, concat_axis=0, tiled=True)  17 us
    all_to_all x1, waiting for transfers between devices, body(): lax.all_to_all(placed.astype(jnp.bfloat16).reshape(experts, capacity, mix...  16.4 us
    all_to_all x1, blocking collectives, summed_on_arrival(): blocks = lax.all_to_all(cut_along(x, dim, length), axis, 0, 0, tiled=True)  16.1 us
    all_to_all x4, starting transfers between devices, from_everyone(): return lax.all_to_all(copies, axis, split_axis=0, concat_axis=0, tiled=True)  15.6 us
  transfers between devices with their start and end apart: 11, of which 9 were waited for; matrix products, arithmetic and copies ran while one was open for 7% of the time, Pallas kernels for 0%

profile of v1, /device:TPU:32, one launch (start us, length us, event | category | flops | bytes accessed | tf_op | source)
XLA Modules:
  0.0 271.6 jit_solution(623000120929470631)
XLA Ops:
  7.2 1.4 broadcast_in_dim.23
  8.7 4.5 %all-to-all-start = ((bf16[4,16,256]{2,1,0:T(8,128)(2,1)}), bf16[4,16,256]{2,1,0:T(8,128)(2,1)S(1)}, u32[]{:S(2)}, u32[]{:S(2)}) async-start(bf16[4,16,256]{2,1,0:T(8,128)(2,1)} %broadcast_in_dim.23), calls=%async_computation | async-start | bytes 65536 | tf_op jit(solution)/shard_map/all_to_all | solution.py:23
  13.1 0.8 copy.76
  14.1 0.7 iota_compare_fusion.4
  14.8 0.7 mul.280
  15.5 0.7 mul.289
  16.3 1.5 copy.74
  20.1 0.2 fusion.25
  20.9 1.3 multiply_reduce_fusion.2
  22.2 0.8 convolution_bitcast_fusion.3
  23.0 4.9 %all-to-all-start.1 = ((f32[4,16,256]{2,1,0:T(8,128)}), f32[4,16,256]{2,1,0:T(8,128)S(1)}, u32[]{:S(2)}, u32[]{:S(2)}) async-start(f32[4,16,256]{2,1,0:T(8,128)} %convolution_bitcast_fusion.3), calls=%async_computation.1 | async-start | bytes 131072 | tf_op jit(solution)/shard_map/all_to_all | solution.py:38
  28.2 5.4 %all-to-all-done.1 = f32[4,16,256]{2,1,0:T(8,128)S(1)} async-done(((f32[4,16,256]{2,1,0:T(8,128)}), f32[4,16,256]{2,1,0:T(8,128)S(1)}, u32[]{:S(2)}, u32[]{:S(2)}) %all-to-all-start.1) | async-done | bytes 65568 | tf_op jit(solution)/shard_map/all_to_all | solution.py:38
  33.8 0.6 broadcast_in_dim.25
  34.4 3.2 %all-to-all-start.2 = ((f32[4,1,32]{2,1,0:T(1,128)}), f32[4,1,32]{2,1,0:T(1,128)S(1)}, u32[]{:S(2)}, u32[]{:S(2)}) async-start(f32[4,1,32]{2,1,0:T(1,128)} %broadcast_in_dim.25), calls=%async_computation.2 | async-start | bytes 4096 | tf_op jit(solution)/shard_map/all_to_all | solution.py:23
  37.6 5.2 %all-to-all-done.2 = f32[4,1,32]{2,1,0:T(1,128)S(1)} async-done(((f32[4,1,32]{2,1,0:T(1,128)}), f32[4,1,32]{2,1,0:T(1,128)S(1)}, u32[]{:S(2)}, u32[]{:S(2)}) %all-to-all-start.2) | async-done | bytes 544 | tf_op jit(solution)/shard_map/all_to_all | solution.py:23
  43.2 0.7 reshape.306
  43.9 19.0 %all-to-all-start.3 = ((bf16[128,2,256]{2,1,0:T(2,128)(2,1)}), bf16[128,2,256]{2,1,0:T(2,128)(2,1)S(1)}, u32[]{:S(2)}, u32[]{:S(2)}) async-start(bf16[128,2,256]{2,1,0:T(2,128)(2,1)} %reshape.306), calls=%async_computation.3 | async-start | bytes 262144 | tf_op jit(solution)/shard_map/all_to_all | solution.py:224
  63.0 0.6 pad_maximum_fusion.2
  63.7 16.4 %all-to-all-done.3 = bf16[128,2,256]{2,1,0:T(2,128)(2,1)S(1)} async-done(((bf16[128,2,256]{2,1,0:T(2,128)(2,1)}), bf16[128,2,256]{2,1,0:T(2,128)(2,1)S(1)}, u32[]{:S(2)}, u32[]{:S(2)}) %all-to-all-start.3) | async-done | bytes 131104 | tf_op jit(solution)/shard_map/all_to_all | solution.py:224
  80.0 1.1 broadcast_in_dim.27
  81.1 3.6 %all-to-all-start.4 = ((bf16[4,128,2,256]{3,2,1,0:T(2,128)(2,1)}), bf16[4,128,2,256]{3,2,1,0:T(2,128)(2,1)S(1)}, u32[]{:S(2)}, u32[]{:S(2)}) async-start(bf16[4,128,2,256]{3,2,1,0:T(2,128)(2,1)} %broadcast_in_dim.27), calls=%async_computation.4 | async-start | bytes 1048576 | tf_op jit(solution)/shard_map/all_to_all | solution.py:23
  84.9 9.8 %all-to-all-done.4 = bf16[4,128,2,256]{3,2,1,0:T(2,128)(2,1)S(1)} async-done(((bf16[4,128,2,256]{3,2,1,0:T(2,128)(2,1)}), bf16[4,128,2,256]{3,2,1,0:T(2,128)(2,1)S(1)}, u32[]{:S(2)}, u32[]{:S(2)}) %all-to-all-start.4) | async-done | bytes 524320 | tf_op jit(solution)/shard_map/all_to_all | solution.py:23
  94.7 0.6 stack.9
  95.3 3.3 %all-to-all-start.8 = ((bf16[4,1,16,256]{3,2,1,0:T(8,128)(2,1)}), bf16[4,1,16,256]{3,2,1,0:T(8,128)(2,1)S(1)}, u32[]{:S(2)}, u32[]{:S(2)}) async-start(bf16[4,1,16,256]{3,2,1,0:T(8,128)(2,1)} %stack.9), calls=%async_computation.8 | async-start | bytes 65536 | tf_op jit(solution)/shard_map/all_to_all | solution.py:69
  98.6 0.7 copy.78
  99.4 0.3 convolution_minimum_fusion
  99.7 0.3 fusion.3
  100.1 0.3 convolution_bitcast_fusion
  100.5 3.5 %all-to-all-done.8 = bf16[4,1,16,256]{3,2,1,0:T(8,128)(2,1)S(1)} async-done(((bf16[4,1,16,256]{3,2,1,0:T(8,128)(2,1)}), bf16[4,1,16,256]{3,2,1,0:T(8,128)(2,1)S(1)}, u32[]{:S(2)}, u32[]{:S(2)}) %all-to-all-start.8) | async-done | bytes 32800 | tf_op jit(solution)/shard_map/all_to_all | solution.py:69
  104.0 16.1 %all_to_all.57 = f32[4,128,2,256]{3,1,2,0:T(8,128)S(1)} all-to-all(f32[4,128,2,256]{3,1,2,0:T(8,128)S(1)} %copy.81), channel_id=1, replica_groups=mesh['ep_0'=16,'ep_1'=4,'ep_2'=2,'tp'=4] {'tp'}, dimensions={0} | all-to-all | bytes 2097152 | tf_op jit(solution)/shard_map/all_to_all | solution.py:38
  120.1 0.8 stack.10
  120.9 3.8 %all-to-all-start.9 = ((bf16[16,4,16,256]{3,2,1,0:T(8,128)(2,1)}), bf16[16,4,16,256]{3,2,1,0:T(8,128)(2,1)S(1)}, u32[]{:S(2)}, u32[]{:S(2)}) async-start(bf16[16,4,16,256]{3,2,1,0:T(8,128)(2,1)} %stack.10), calls=%async_computation.9 | async-start | bytes 1048576 | tf_op jit(solution)/shard_map/all_to_all | solution.py:69
  124.8 0.8 copy.83
  125.6 24.6 %all-to-all-done.9 = bf16[16,4,16,256]{3,2,1,0:T(8,128)(2,1)S(1)} async-done(((bf16[16,4,16,256]{3,2,1,0:T(8,128)(2,1)}), bf16[16,4,16,256]{3,2,1,0:T(8,128)(2,1)S(1)}, u32[]{:S(2)}, u32[]{:S(2)}) %all-to-all-start.9) | async-done | bytes 524320 | tf_op jit(solution)/shard_map/all_to_all | solution.py:69
  150.2 1.1 pad_maximum_fusion
  151.3 3.6 %all-to-all-start.10 = ((bf16[2,64,16,256]{3,2,1,0:T(8,128)(2,1)}), bf16[2,64,16,256]{3,2,1,0:T(8,128)(2,1)S(1)}, u32[]{:S(2)}, u32[]{:S(2)}) async-start(bf16[2,64,16,256]{3,2,1,0:T(8,128)(2,1)} %pad_maximum_fusion), calls=%async_computation.10 | async-start | bytes 2097152 | tf_op jit(solution)/shard_map/all_to_all | solution.py:69
  154.8 54.1 %all-gather.2.cloned.1.call-done = bf16[2048,512]{1,0:T(8,128)(2,1)} async-done(((bf16[16,512]{1,0:T(8,128)(2,1)}), bf16[2048,512]{1,0:T(8,128)(2,1)}) %all-gather.2.cloned.1.call-update) | async-done | bytes 2097168 | tf_op jit(solution)/shard_map/all_gather | solution.py:57
  208.9 1.6 convolution_bitcast_fusion.2
  210.5 1.6 convolution_bitcast_fusion.1
  212.2 12.2 %all-to-all-start.6 = ((bf16[128,2,256]{2,1,0:T(2,128)(2,1)}), bf16[128,2,256]{2,1,0:T(2,128)(2,1)S(1)}, u32[]{:S(2)}, u32[]{:S(2)}) async-start(bf16[128,2,256]{2,1,0:T(2,128)(2,1)} %copy.83), calls=%async_computation.6 | async-start | bytes 262144 | tf_op jit(solution)/shard_map/all_to_all | solution.py:242
  224.5 17.0 %all-to-all-done.6 = bf16[128,2,256]{2,1,0:T(2,128)(2,1)S(1)} async-done(((bf16[128,2,256]{2,1,0:T(2,128)(2,1)}), bf16[128,2,256]{2,1,0:T(2,128)(2,1)S(1)}, u32[]{:S(2)}, u32[]{:S(2)}) %all-to-all-start.6) | async-done | bytes 131104 | tf_op jit(solution)/shard_map/all_to_all | solution.py:242
  241.6 1.6 broadcast_in_dim.28
  243.1 4.3 %all-to-all-start.7 = ((f32[4,1,65536]{2,1,0:T(1,128)}), f32[4,1,65536]{2,1,0:T(1,128)S(1)}, u32[]{:S(2)}, u32[]{:S(2)}) async-start(f32[4,1,65536]{2,1,0:T(1,128)} %broadcast_in_dim.28), calls=%async_computation.7 | async-start | bytes 2097152 | tf_op jit(solution)/shard_map/all_to_all | solution.py:23
  247.8 0.6 multiply_convert_fusion.6
  248.4 1.1 copy.86
  249.7 13.0 %all-to-all-done.7 = f32[4,1,65536]{2,1,0:T(1,128)S(1)} async-done(((f32[4,1,65536]{2,1,0:T(1,128)}), f32[4,1,65536]{2,1,0:T(1,128)S(1)}, u32[]{:S(2)}, u32[]{:S(2)}) %all-to-all-start.7) | async-done | bytes 1048608 | tf_op jit(solution)/shard_map/all_to_all | solution.py:23
  262.8 1.0 reduce_sum.139
  263.9 0.9 fusion.6
  (101 shorter events, 4.4 us)
Async XLA Ops:
  7.2 13.4 %copy-start = (bf16[16,256,128]{2,1,0:T(8,128)(2,1)S(1)}, bf16[16,256,128]{2,1,0:T(8,128)(2,1)}, u32[]{:S(2)}) copy-start(bf16[16,256,128]{2,1,0:T(8,128)(2,1)} %param.34) | copy-start | bytes 3145732
  7.2 11.2 %copy-start.6 = (bf16[128,1024]{1,0:T(8,128)(2,1)S(1)}, bf16[128,1024]{1,0:T(8,128)(2,1)}, u32[]{:S(2)}) copy-start(bf16[128,1024]{1,0:T(8,128)(2,1)} %param.32) | copy-start | bytes 786436
  7.2 11.7 %copy-start.13 = (f32[1024]{0:T(1024)S(1)}, f32[1024]{0:T(1024)}, u32[]{:S(2)}) copy-start(f32[1024]{0:T(1024)} %param.24) | copy-start | bytes 12292
  7.2 11.8 %copy-start.4 = (bf16[1024,128]{1,0:T(8,128)(2,1)S(1)}, bf16[1024,128]{1,0:T(8,128)(2,1)}, u32[]{:S(2)}) copy-start(bf16[1024,128]{1,0:T(8,128)(2,1)} %param.25) | copy-start | bytes 786436
  7.2 12.1 %copy-start.5 = (bf16[1024,128]{1,0:T(8,128)(2,1)S(1)}, bf16[1024,128]{1,0:T(8,128)(2,1)}, u32[]{:S(2)}) copy-start(bf16[1024,128]{1,0:T(8,128)(2,1)} %param.26) | copy-start | bytes 786436
  8.7 10.1 %all-to-all-start = ((bf16[4,16,256]{2,1,0:T(8,128)(2,1)}), bf16[4,16,256]{2,1,0:T(8,128)(2,1)S(1)}, u32[]{:S(2)}, u32[]{:S(2)}) async-start(bf16[4,16,256]{2,1,0:T(8,128)(2,1)} %broadcast_in_dim.23), calls=%async_computation | async-start | bytes 65536 | tf_op jit(solution)/shard_map/all_to_all | solution.py:23
  18.6 3.6 %copy-start.16 = (f32[128]{0:T(128)S(1)}, f32[128]{0:T(128)}, u32[]{:S(2)}) copy-start(f32[128]{0:T(128)} %param.31) | copy-start | bytes 1540
  18.9 9.2 %copy-start.14 = (f32[256]{0:T(256)S(1)}, f32[256]{0:T(256)}, u32[]{:S(2)}) copy-start(f32[256]{0:T(256)} %param.36) | copy-start | bytes 3076
  18.9 9.3 %copy-start.15 = (f32[256]{0:T(256)S(1)}, f32[256]{0:T(256)}, u32[]{:S(2)}) copy-start(f32[256]{0:T(256)} %param.45) | copy-start | bytes 3076
  19.0 14.6 %copy-start.7 = (bf16[16,256]{1,0:T(8,128)(2,1)S(1)}, bf16[16,256]{1,0:T(8,128)(2,1)}, u32[]{:S(2)}) copy-start(bf16[16,256]{1,0:T(8,128)(2,1)} %param.23) | copy-start | bytes 24580
  20.1 42.8 %copy-start.10 = (bf16[256,16]{0,1:T(8,128)(2,1)S(1)}, bf16[256,16]{0,1:T(8,128)(2,1)}, u32[]{:S(2)}) copy-start(bf16[256,16]{0,1:T(8,128)(2,1)} %param.43) | copy-start | bytes 24580
  20.1 42.9 %copy-start.11 = (bf16[256,16]{0,1:T(8,128)(2,1)S(1)}, bf16[256,16]{0,1:T(8,128)(2,1)}, u32[]{:S(2)}) copy-start(bf16[256,16]{0,1:T(8,128)(2,1)} %param.42) | copy-start | bytes 24580
  20.9 63.9 %copy-start.2 = (bf16[1,256,1024]{2,1,0:T(8,128)(2,1)S(1)}, bf16[1,256,1024]{2,1,0:T(8,128)(2,1)}, u32[]{:S(2)}) copy-start(bf16[1,256,1024]{2,1,0:T(8,128)(2,1)} %param.41) | copy-start | bytes 1572868
  22.2 62.8 %copy-start.12 = (bf16[16,128]{1,0:T(8,128)(2,1)}, bf16[16,128]{1,0:T(8,128)(2,1)S(1)}, u32[]{:S(2)}) copy-start(bf16[16,128]{1,0:T(8,128)(2,1)S(1)} %get-tuple-element.18) | copy-start | bytes 12292
  23.0 71.7 %copy-start.9 = (bf16[16,256]{1,0:T(8,128)(2,1)S(1)}, bf16[16,256]{1,0:T(8,128)(2,1)}, u32[]{:S(2)}) copy-start(bf16[16,256]{1,0:T(8,128)(2,1)} %param.44) | copy-start | bytes 24580
  23.0 10.6 %all-to-all-start.1 = ((f32[4,16,256]{2,1,0:T(8,128)}), f32[4,16,256]{2,1,0:T(8,128)S(1)}, u32[]{:S(2)}, u32[]{:S(2)}) async-start(f32[4,16,256]{2,1,0:T(8,128)} %convolution_bitcast_fusion.3), calls=%async_computation.1 | async-start | bytes 131072 | tf_op jit(solution)/shard_map/all_to_all | solution.py:38
  34.4 8.4 %all-to-all-start.2 = ((f32[4,1,32]{2,1,0:T(1,128)}), f32[4,1,32]{2,1,0:T(1,128)S(1)}, u32[]{:S(2)}, u32[]{:S(2)}) async-start(f32[4,1,32]{2,1,0:T(1,128)} %broadcast_in_dim.25), calls=%async_computation.2 | async-start | bytes 4096 | tf_op jit(solution)/shard_map/all_to_all | solution.py:23
  43.9 36.1 %all-to-all-start.3 = ((bf16[128,2,256]{2,1,0:T(2,128)(2,1)}), bf16[128,2,256]{2,1,0:T(2,128)(2,1)S(1)}, u32[]{:S(2)}, u32[]{:S(2)}) async-start(bf16[128,2,256]{2,1,0:T(2,128)(2,1)} %reshape.306), calls=%async_computation.3 | async-start | bytes 262144 | tf_op jit(solution)/shard_map/all_to_all | solution.py:224
  62.9 146.0 %all-gather.2.cloned.1.call-start = ((), (), s32[]{:S(2)}) async-start(), calls=%async_computation.11 | async-start | bytes 2113536 | tf_op jit(solution)/shard_map/all_gather | solution.py:57
  81.1 18.3 %copy-start.3 = (bf16[1,1024,256]{2,1,0:T(8,128)(2,1)S(1)}, bf16[1,1024,256]{2,1,0:T(8,128)(2,1)}, u32[]{:S(2)}) copy-start(bf16[1,1024,256]{2,1,0:T(8,128)(2,1)} %param.39) | copy-start | bytes 1572868
  81.1 13.6 %all-to-all-start.4 = ((bf16[4,128,2,256]{3,2,1,0:T(2,128)(2,1)}), bf16[4,128,2,256]{3,2,1,0:T(2,128)(2,1)S(1)}, u32[]{:S(2)}, u32[]{:S(2)}) async-start(bf16[4,128,2,256]{3,2,1,0:T(2,128)(2,1)} %broadcast_in_dim.27), calls=%async_computation.4 | async-start | bytes 1048576 | tf_op jit(solution)/shard_map/all_to_all | solution.py:23
  84.9 14.8 %copy-start.18 = (bf16[1,1024,256]{2,1,0:T(8,128)(2,1)S(1)}, bf16[1,1024,256]{2,1,0:T(8,128)(2,1)}, u32[]{:S(2)}) copy-start(bf16[1,1024,256]{2,1,0:T(8,128)(2,1)} %param.40) | copy-start | bytes 1572868
  95.3 8.7 %all-to-all-start.8 = ((bf16[4,1,16,256]{3,2,1,0:T(8,128)(2,1)}), bf16[4,1,16,256]{3,2,1,0:T(8,128)(2,1)S(1)}, u32[]{:S(2)}, u32[]{:S(2)}) async-start(bf16[4,1,16,256]{3,2,1,0:T(8,128)(2,1)} %stack.9), calls=%async_computation.8 | async-start | bytes 65536 | tf_op jit(solution)/shard_map/all_to_all | solution.py:69
  120.9 29.3 %all-to-all-start.9 = ((bf16[16,4,16,256]{3,2,1,0:T(8,128)(2,1)}), bf16[16,4,16,256]{3,2,1,0:T(8,128)(2,1)S(1)}, u32[]{:S(2)}, u32[]{:S(2)}) async-start(bf16[16,4,16,256]{3,2,1,0:T(8,128)(2,1)} %stack.10), calls=%async_computation.9 | async-start | bytes 1048576 | tf_op jit(solution)/shard_map/all_to_all | solution.py:69
  151.3 60.9 %all-to-all-start.10 = ((bf16[2,64,16,256]{3,2,1,0:T(8,128)(2,1)}), bf16[2,64,16,256]{3,2,1,0:T(8,128)(2,1)S(1)}, u32[]{:S(2)}, u32[]{:S(2)}) async-start(bf16[2,64,16,256]{3,2,1,0:T(8,128)(2,1)} %pad_maximum_fusion), calls=%async_computation.10 | async-start | bytes 2097152 | tf_op jit(solution)/shard_map/all_to_all | solution.py:69
  212.2 35.3 %copy-start.8 = (f32[16,6]{0,1:T(8,128)S(1)}, f32[16,6]{0,1:T(8,128)}, u32[]{:S(2)}) copy-start(f32[16,6]{0,1:T(8,128)} %param.38) | copy-start | bytes 1156
  212.2 29.3 %all-to-all-start.6 = ((bf16[128,2,256]{2,1,0:T(2,128)(2,1)}), bf16[128,2,256]{2,1,0:T(2,128)(2,1)S(1)}, u32[]{:S(2)}, u32[]{:S(2)}) async-start(bf16[128,2,256]{2,1,0:T(2,128)(2,1)} %copy.83), calls=%async_computation.6 | async-start | bytes 262144 | tf_op jit(solution)/shard_map/all_to_all | solution.py:242
  224.5 23.3 %copy-start.17 = (f32[128]{0:T(128)S(1)}, f32[128]{0:T(128)}, u32[]{:S(2)}) copy-start(f32[128]{0:T(128)} %param.29) | copy-start | bytes 1540
  243.1 19.7 %all-to-all-start.7 = ((f32[4,1,65536]{2,1,0:T(1,128)}), f32[4,1,65536]{2,1,0:T(1,128)S(1)}, u32[]{:S(2)}, u32[]{:S(2)}) async-start(f32[4,1,65536]{2,1,0:T(1,128)} %broadcast_in_dim.28), calls=%async_computation.7 | async-start | bytes 2097152 | tf_op jit(solution)/shard_map/all_to_all | solution.py:23
  249.5 14.3 %copy-start.1 = (bf16[2,64,16,256]{3,2,0,1:T(8,128)(2,1)S(1)}, bf16[2,64,16,256]{3,2,0,1:T(8,128)(2,1)}, u32[]{:S(2)}) copy-start(bf16[2,64,16,256]{3,2,0,1:T(8,128)(2,1)} %copy.86) | copy-start | bytes 3145732
Sparse Core Ops, SparseCore 0:
  66.9 141.9 all-gather.1
